TPU v7x, 128 devices: a whole 4x4x4 slice. The times are simulated.
128 devices in a mesh: kv: 16 (over z, y), tp: 8 (over x, core).
Axes of the slice: x: 4, y: 4, z: 4, core: 2. Of those that a mesh axis runs over, the one named last changes fastest.
Arguments:
- tokens: bfloat16 [256, 4096], P(None, ('kv', 'tp')), may hold values from -64 to 64
- mix_gain: float32 [4096], P('kv'), may hold values from 0.1 to 1.9
- w_query: bfloat16 [4096, 3072], P('kv', 'tp'), may hold values from -0.09375 to 0.09375
- w_key: bfloat16 [4096, 3072], P('kv', 'tp'), may hold values from -0.09375 to 0.09375
- w_value: bfloat16 [4096, 3072], P('kv', 'tp'), may hold values from -0.09375 to 0.09375
- w_gate: bfloat16 [4096, 3072], P('kv', 'tp'), may hold values from -0.09375 to 0.09375
- w_beta: bfloat16 [4096, 24], P('kv'), may hold values from -0.09375 to 0.09375
- w_decay: bfloat16 [4096, 24], P('kv'), may hold values from -0.09375 to 0.09375
- decay_rate: float32 [24], P('tp'), may hold values from 0.15 to 1.5
- out_gain: float32 [128], replicated, may hold values from 0.1 to 1.9
- state: float32 [256, 24, 128, 128], P('kv', 'tp'), may hold values from -0.6 to 0.6
- w_out: bfloat16 [3072, 4096], P('tp', 'kv'), may hold values from -0.109375 to 0.109375
- mlp_gain: float32 [4096], replicated, may hold values from 0.1 to 1.9
- w_up: bfloat16 [4096, 16384], P(None, ('kv', 'tp')), may hold values from -0.09375 to 0.09375
- w_down: bfloat16 [16384, 4096], P(('kv', 'tp')), may hold values from -0.1875 to 0.1875
Outputs:
- mixed: bfloat16 [256, 4096], P(None, ('kv', 'tp'))
- new_state: float32 [256, 24, 128, 128], P('kv', 'tp')
All inputs are finite; a program needn't handle non-finite values.
Results may differ from a plain program's by a relative error of at most 0.0063.
Values may be sent and summed in bfloat16 or wider, within the bound.
A program may use at most 64 MiB of HBM per device.

v0:
```python
import math
import jax
import jax.numpy as jnp
from jax import lax
from jax.sharding import Mesh
from jax.sharding import PartitionSpec as P

D = 4096
TP = ("tp_0", "tp_1")
KV = ("kv_0", "kv_1")
KV_TP = ("kv_0", "kv_1", "tp_0", "tp_1")
EPSILON = 1e-06


def side_by_side(arrays, axis, dim, along):
    widths = [math.prod(a.shape[along:]) for a in arrays]
    both = jnp.concatenate(
        [a.reshape(*a.shape[:along], w) for a, w in zip(arrays, widths)], axis=along
    )
    filled = lax.psum_scatter(both, axis, scatter_dimension=dim, tiled=True)
    pieces = jnp.split(filled, [sum(widths[:k]) for k in range(1, len(widths))], axis=along)
    return tuple(
        (b.reshape(*filled.shape[:along], *a.shape[along:]) for a, b in zip(arrays, pieces))
    )


def in_blocks(value, dim, count):
    shape = value.shape
    pieces = value.reshape(*shape[:dim], count, shape[dim] // count, *shape[dim + 1 :])
    return jnp.moveaxis(pieces, dim, 0)


def summed_on_arrival(value, axis, dim):
    count = lax.axis_size(axis)
    pieces = lax.all_to_all(in_blocks(value, dim, count), axis, 0, 0, tiled=True)
    return jnp.sum(pieces, axis=0)


def joined_along(pieces, dim):
    shape = list(pieces.shape[1:])
    shape[dim] *= pieces.shape[0]
    return jnp.moveaxis(pieces, 0, dim).reshape(shape)


def exchange_in_order(pieces, axes, sequence):
    inside = pieces.shape[1:]
    filled = pieces.reshape(*(lax.axis_size(a) for a in axes), *inside)
    for k in sequence:
        filled = lax.all_to_all(filled, axes[k], k, k, tiled=True)
    return filled.reshape(-1, *inside)


def exchange_by_chip(value, groups, sequence, split_dim, concat_dim):
    count = lax.axis_size(groups[0]) * lax.axis_size(groups[1])
    pieces = in_blocks(value, split_dim, count)
    return joined_along(exchange_in_order(pieces, groups, sequence), concat_dim)


def head_norm(values):
    return values * lax.rsqrt(jnp.sum(values * values, axis=-1, keepdims=True) + EPSILON)


def feed_forward(segment, mlp_gain, w_up, w_down):
    segment_f = segment.astype(jnp.float32)
    normed_mlp = (
        segment_f
        * lax.rsqrt(jnp.mean(segment_f * segment_f, axis=1, keepdims=True) + EPSILON)
        * mlp_gain[None, :]
    ).astype(jnp.bfloat16)
    hidden = jnp.square(
        jax.nn.relu(jnp.dot(normed_mlp, w_up, preferred_element_type=jnp.float32))
    ).astype(jnp.bfloat16)
    return jnp.dot(hidden, w_down, preferred_element_type=jnp.float32)


def local(
    tokens,
    mix_gain,
    w_query,
    w_key,
    w_value,
    w_gate,
    w_beta,
    w_decay,
    decay_rate,
    out_gain,
    state,
    w_out,
    mlp_gain,
    w_up,
    w_down,
):
    local_rows = state.shape[0]
    local_heads = decay_rate.shape[0]
    head_size = state.shape[2]
    all_heads = w_beta.shape[1]
    columns = lax.all_gather(tokens, TP, axis=1, tiled=True)
    columns_f = columns.astype(jnp.float32)
    normed = (columns_f * mix_gain[None, :]).astype(jnp.bfloat16)
    part_query = jnp.dot(normed, w_query, preferred_element_type=jnp.float32)
    part_key = jnp.dot(normed, w_key, preferred_element_type=jnp.float32)
    part_value = jnp.dot(normed, w_value, preferred_element_type=jnp.float32)
    part_gate = jnp.dot(normed, w_gate, preferred_element_type=jnp.float32)
    part_rates = jnp.dot(
        normed, jnp.concatenate([w_beta, w_decay], axis=1), preferred_element_type=jnp.float32
    )
    summed = side_by_side(
        (
            part_query,
            part_key,
            part_value,
            part_gate,
            part_rates,
            jnp.sum(columns_f * columns_f, axis=1),
        ),
        KV,
        0,
        1,
    )
    own_squares = summed[5]
    row_scale = lax.rsqrt(own_squares / D + EPSILON)[:, None]
    shape_heads = (local_rows, local_heads, head_size)
    query = head_norm(jax.nn.silu((summed[0] * row_scale).reshape(shape_heads))) * head_size ** (
        -0.5
    )
    key = head_norm(jax.nn.silu((summed[1] * row_scale).reshape(shape_heads)))
    value = jax.nn.silu((summed[2] * row_scale).reshape(shape_heads))
    gate_raw = (summed[3] * row_scale).reshape(shape_heads)
    rates = summed[4] * row_scale
    head_start = lax.axis_index(TP) * local_heads
    beta = jax.nn.sigmoid(lax.dynamic_slice_in_dim(rates, head_start, local_heads, 1))
    decay_raw = lax.dynamic_slice_in_dim(rates, all_heads + head_start, local_heads, 1)
    decay = jnp.exp(-decay_rate[None, :] * jax.nn.softplus(decay_raw))
    faded = state * decay[:, :, None, None]
    recalled = jnp.einsum("bhkv,bhk->bhv", faded, key, precision=lax.Precision.HIGHEST)
    change = beta[:, :, None] * (value - recalled)
    new_state = faded + key[:, :, :, None] * change[:, :, None, :]
    readout = jnp.einsum("bhkv,bhk->bhv", new_state, query, precision=lax.Precision.HIGHEST)
    scaled = (
        readout
        * lax.rsqrt(jnp.mean(readout * readout, axis=-1, keepdims=True) + EPSILON)
        * out_gain
    )
    merged = (
        (scaled * jax.nn.silu(gate_raw))
        .reshape(local_rows, local_heads * head_size)
        .astype(jnp.bfloat16)
    )
    partial_out = jnp.dot(
        lax.all_gather(merged, KV, axis=0, tiled=True), w_out, preferred_element_type=jnp.float32
    )
    branch_sum = summed_on_arrival(partial_out, TP, 1)
    residual = (tokens.astype(jnp.float32) + branch_sum).astype(jnp.bfloat16)
    whole_rows = lax.all_gather(residual, KV_TP, axis=1, tiled=True)
    partial_mlp = feed_forward(whole_rows, mlp_gain, w_up, w_down)
    row_branch = lax.psum_scatter(partial_mlp, KV_TP, scatter_dimension=0, tiled=True)
    own_count = row_branch.shape[0]
    own_rows = lax.dynamic_slice_in_dim(whole_rows, lax.axis_index(KV_TP) * own_count, own_count, 0)
    finished = (own_rows.astype(jnp.float32) + row_branch).astype(jnp.bfloat16)
    mixed = exchange_by_chip(finished, (("kv_0", "kv_1", "tp_0"), "tp_1"), (1, 0), 1, 0)
    return (mixed, new_state)


def solution(mesh):
    torus = Mesh(mesh.devices.reshape(4, 4, 4, 2), ("kv_0", "kv_1", "tp_0", "tp_1"))
    in_specs = (
        P(None, KV_TP),
        P(KV),
        P(KV, TP),
        P(KV, TP),
        P(KV, TP),
        P(KV, TP),
        P(KV, None),
        P(KV, None),
        P(TP),
        P(),
        P(KV, TP, None, None),
        P(TP, KV),
        P(),
        P(None, KV_TP),
        P(KV_TP, None),
    )
    out_specs = (P(None, KV_TP), P(KV, TP, None, None))
    return jax.shard_map(local, mesh=torus, in_specs=in_specs, out_specs=out_specs, check_vma=False)
```

profile of v0, /device:TPU:0, one launch (start us, length us, event | category | flops | bytes accessed | tf_op | source)
XLA Modules:
  0.0 419.6 jit_solution(876211718287899662)
XLA Ops:
  7.3 13.6 %all_gather.9 = bf16[256,256]{0,1:T(8,128)(2,1)S(1)} all-gather(bf16[256,32]{0,1:T(8,128)(2,1)} %param.15), channel_id=1, replica_groups=mesh['kv_0'=4,'kv_1'=4,'tp_0'=4,'tp_1'=2] {'tp_0','tp_1'}, dimensions={1}, use_global_device_ids=true | all-gather | bytes 147456 | tf_op jit(solution)/shard_map/all_gather | solution.py:97
  20.8 0.1 fusion.23
  20.9 0.1 copy.42
  21.0 1.3 fusion.51
  22.3 1.3 fusion.49
  23.6 1.3 fusion.47
  24.9 1.3 fusion.53
  26.2 0.3 fusion.32
  26.5 1.4 concatenate.7
  27.9 0.0 all-gather.2.cloned.1.call-start
  28.0 0.6 dynamic-slice
  29.3 89.5 %all-reduce.5.cloned.1.call-done = f32[256,1585]{1,0:T(8,128)} async-done(((f32[256,1585]{1,0:T(8,128)}), f32[256,1585]{1,0:T(8,128)}) %all-reduce.5.cloned.1.call-update) | async-done | bytes 1623056
  118.8 0.9 fusion.43
  119.7 0.9 dynamic-slice_multiply_fusion.1
  120.6 0.1 multiply_reduce_fusion.1
  120.8 0.1 fusion.65
  120.8 0.1 broadcast_multiply_fusion
  121.0 0.1 multiply_reduce_fusion
  121.1 0.1 multiply_bitcast_fusion
  121.2 0.9 dynamic-slice_multiply_fusion.5
  122.1 0.1 add_divide_fusion
  122.3 4.8 %fusion.3 = f32[16,3,1,128]{3,2,1,0:T(1,128)S(1)} fusion(f32[16,3,128,128]{3,2,1,0:T(8,128)} %param.25, f32[16,3]{1,0:T(8,128)S(1)} %get-tuple-element.15, f32[16,3,128,1]{2,1,0,3:T(4,128)S(1)} %fusion.65), kind=kOutput, calls=%fused_computation.6 | convolution fusion | flops 10223616 | bytes 3195072 | tf_op jit(solution)/shard_map/bhkv,bhk->bhv/dot_general | solution.py:135
  127.0 0.1 fusion.30
  127.1 1.1 multiply_add_fusion
  128.3 1.7 copy-done.3
  129.9 2.8 fusion.36
  132.7 0.1 fusion.28
  132.8 0.1 fusion.31
  132.9 23.2 %all_gather.10 = bf16[256,384]{1,0:T(8,128)(2,1)S(1)} all-gather(bf16[16,384]{1,0:T(8,128)(2,1)S(1)} %bitcast.49), channel_id=1, replica_groups=mesh['kv_0'=4,'kv_1'=4,'tp_0'=4,'tp_1'=2] {'kv_0','kv_1'}, dimensions={0}, use_global_device_ids=true | all-gather | bytes 208896 | tf_op jit(solution)/shard_map/all_gather | solution.py:150
  156.1 0.3 fusion.55
  156.4 11.6 %all_to_all.15 = f32[8,256,32]{1,2,0:T(8,128)S(1)} all-to-all(f32[8,256,32]{1,2,0:T(8,128)S(1)} %bitcast.43), channel_id=1, replica_groups=mesh['kv_0'=4,'kv_1'=4,'tp_0'=4,'tp_1'=2] {'tp_0','tp_1'}, dimensions={0} | all-to-all | bytes 524288 | tf_op jit(solution)/shard_map/all_to_all | solution.py:35
  168.0 0.6 add_convert_fusion
  168.7 0.2 all-reduce.7.cloned.1.call-start
  168.9 61.9 %all-gather.2.cloned.1.call-done = bf16[256,4096]{0,1:T(8,128)(2,1)} async-done(((bf16[256,32]{0,1:T(8,128)(2,1)}), bf16[256,4096]{0,1:T(8,128)(2,1)}) %all-gather.2.cloned.1.call-update) | async-done | bytes 2097168 | tf_op jit(solution)/shard_map/all_gather | solution.py:154
  230.8 2.3 fusion
  233.2 5.3 %fusion.20 = f32[256,4096]{1,0:T(8,128)} fusion(bf16[128,4096]{1,0:T(8,128)(2,1)S(1)} %copy-done, bf16[4096,128]{1,0:T(8,128)(2,1)} %param.28, bf16[256,4096]{0,1:T(8,128)(2,1)S(1)} %copy-done.1, f32[4096]{0:T(1024)S(1)} %copy-done.7, f32[256]{0:T(256)S(1)} %add_rsqrt_fusion.3), kind=kOutput, calls=%fused_computation.15 | convolution fusion | flops 541163520 | bytes 8406016 | tf_op jit(solution)/shard_map/dot_general | solution.py:73
  238.5 1.4 constant_dynamic-slice_fusion
  240.0 1.6 copy.52
  241.6 148.9 %all-reduce.7.cloned.1.call-done = f32[256,4096]{1,0:T(8,128)} async-done(((f32[256,4096]{1,0:T(8,128)}), f32[256,4096]{1,0:T(8,128)}) %all-reduce.7.cloned.1.call-update) | async-done | bytes 4194320
  390.5 0.9 fusion.27
  391.4 0.1 reshape.86
  391.5 0.1 copy.44
  391.6 0.1 reshape.94
  391.7 3.7 all_to_all.16
  395.4 0.1 reshape.95
  395.5 0.1 copy.45
  395.6 16.7 %all_to_all.17 = bf16[64,2,2,32]{3,2,1,0:T(2,128)(2,1)S(1)} all-to-all(bf16[64,2,2,32]{3,2,1,0:T(2,128)(2,1)S(1)} %copy.45), channel_id=1, replica_groups=mesh['kv_0'=4,'kv_1'=4,'tp_0'=4,'tp_1'=2] {'kv_0','kv_1','tp_0'}, dimensions={0} | all-to-all | bytes 32768 | tf_op jit(solution)/shard_map/all_to_all | solution.py:49
  412.3 0.7 copy.46
  (40 shorter events, 0.3 us)
Async XLA Ops:
  7.2 226.0 %copy-start = (bf16[128,4096]{1,0:T(8,128)(2,1)S(1)}, bf16[128,4096]{1,0:T(8,128)(2,1)}, u32[]{:S(2)}) copy-start(bf16[128,4096]{1,0:T(8,128)(2,1)} %param.29) | copy-start | bytes 3145732
  7.2 19.0 %copy-start.6 = (f32[256]{0:T(256)S(1)}, f32[256]{0:T(256)}, u32[]{:S(2)}) copy-start(f32[256]{0:T(256)} %param.16) | copy-start | bytes 3076
  7.2 19.0 %copy-start.8 = (bf16[256,24]{0,1:T(8,128)(2,1)S(1)}, bf16[256,24]{0,1:T(8,128)(2,1)}, u32[]{:S(2)}) copy-start(bf16[256,24]{0,1:T(8,128)(2,1)} %param.22) | copy-start | bytes 36868
  7.2 19.0 %copy-start.9 = (bf16[256,24]{0,1:T(8,128)(2,1)S(1)}, bf16[256,24]{0,1:T(8,128)(2,1)}, u32[]{:S(2)}) copy-start(bf16[256,24]{0,1:T(8,128)(2,1)} %param.21) | copy-start | bytes 36868
  7.2 111.6 %all-reduce.5.cloned.1.call-start = ((), (), s32[]{:S(2)}) async-start(), calls=%async_computation.4 | async-start | bytes 3407872
  24.9 3.2 copy-start.11
  24.9 3.2 copy-start.12
  27.9 202.9 %all-gather.2.cloned.1.call-start = ((), (), s32[]{:S(2)}) async-start(), calls=%async_computation.3 | async-start | bytes 2113536 | tf_op jit(solution)/shard_map/all_gather | solution.py:154
  121.2 5.9 %copy-start.2 = (f32[16,3,128,128]{3,2,1,0:T(8,128)S(1)}, f32[16,3,128,128]{3,2,1,0:T(8,128)}, u32[]{:S(2)}) copy-start(f32[16,3,128,128]{3,2,1,0:T(8,128)} %param.25) | copy-start | bytes 9437188
  128.3 1.7 copy-start.3
  129.9 2.9 copy-start.10
  129.9 26.2 %copy-start.4 = (bf16[384,256]{1,0:T(8,128)(2,1)S(1)}, bf16[384,256]{1,0:T(8,128)(2,1)}, u32[]{:S(2)}) copy-start(bf16[384,256]{1,0:T(8,128)(2,1)} %param.26) | copy-start | bytes 589828
  129.9 38.1 %copy-start.5 = (bf16[256,32]{0,1:T(8,128)(2,1)S(1)}, bf16[256,32]{0,1:T(8,128)(2,1)}, u32[]{:S(2)}) copy-start(bf16[256,32]{0,1:T(8,128)(2,1)} %param.15) | copy-start | bytes 49156
  129.9 103.2 %copy-start.7 = (f32[4096]{0:T(1024)S(1)}, f32[4096]{0:T(1024)}, u32[]{:S(2)}) copy-start(f32[4096]{0:T(1024)} %param.27) | copy-start | bytes 49156
  168.7 221.8 %all-reduce.7.cloned.1.call-start = ((), (), s32[]{:S(2)}) async-start(), calls=%async_computation.5 | async-start | bytes 8388608
  230.8 2.3 copy-start.1
Sparse Core Ops, SparseCore 0:
  28.1 90.6 all-reduce.4
  168.8 62.0 all-gather.1
  238.7 151.7 all-reduce.6
where the time goes:
time: 420 us
  waiting for transfers between devices  300 us (71%)
  blocking collectives  68.7 us (16%)
  matrix products  18.6 us (4%)
  between operations  14.8 us (4%)
  other arithmetic  8.67 us (2%)
  local copies, waits for them, and re-layouts  8.14 us (2%)
    unnamed x5, waiting for transfers between devices  238 us
    all_gather x1, waiting for transfers between devices, local(): whole_rows = lax.all_gather(residual, KV_TP, axis=1, tiled=True)  61.9 us
    all_gather x1, blocking collectives, local(): lax.all_gather(merged, KV, axis=0, tiled=True)  23.2 us
    all_to_all x2, blocking collectives, exchange_in_order(): filled = lax.all_to_all(filled, axes[k], k, k, tiled=True)  20.4 us
    all_gather x1, blocking collectives, local(): columns = lax.all_gather(tokens, TP, axis=1, tiled=True)  13.6 us
    all_to_all x1, blocking collectives, summed_on_arrival(): lax.all_to_all(in_blocks(value, dim, count), axis, 0, 0, tiled=True)  11.6 us
  transfers between devices with their start and end apart: 3, of which 3 were waited for; matrix products, arithmetic and copies ran while one was open for 1% of the time, Pallas kernels for 0%

commit v1 on v0

--- a/solution.py
+++ b/solution.py
@@ -1,15 +1,25 @@
+import functools
 import math
 import jax
 import jax.numpy as jnp
 from jax import lax
 from jax.sharding import Mesh
 from jax.sharding import PartitionSpec as P
+from jax.lax import all_to_all, axis_size
 
 D = 4096
 TP = ("tp_0", "tp_1")
 KV = ("kv_0", "kv_1")
 KV_TP = ("kv_0", "kv_1", "tp_0", "tp_1")
 EPSILON = 1e-06
+
+
+def cover_run(my_tile, where_dim):
+    r1 = all_to_all(jnp.stack(axis_size(KV) * [my_tile]), concat_axis=0, split_axis=0, axis_name=KV)
+    return jnp.concatenate(r1, where_dim)
+
+
+unite_sectors = functools.partial(cover_run, where_dim=0)
 
 
 def side_by_side(arrays, axis, dim, along):
@@ -146,9 +156,7 @@
         .reshape(local_rows, local_heads * head_size)
         .astype(jnp.bfloat16)
     )
-    partial_out = jnp.dot(
-        lax.all_gather(merged, KV, axis=0, tiled=True), w_out, preferred_element_type=jnp.float32
-    )
+    partial_out = jnp.dot(unite_sectors(merged), w_out, preferred_element_type=jnp.float32)
     branch_sum = summed_on_arrival(partial_out, TP, 1)
     residual = (tokens.astype(jnp.float32) + branch_sum).astype(jnp.bfloat16)
     whole_rows = lax.all_gather(residual, KV_TP, axis=1, tiled=True)

time: 420 us -> 410 us (0.976)
  blocking collectives: 68.7 us -> 45.5 us
  waiting for transfers between devices: 300 us -> 308 us
  starting transfers between devices: 0.3 us -> 5.42 us
    all_gather x1 -> x0, blocking collectives: 23.2 us -> none  [local(): lax.all_gather(merged, KV, axis=0, tiled=True)]
    all_to_all x0 -> x1, waiting for transfers between devices: none -> 8.11 us  [cover_run(): all_to_all(jnp.stack(axis_size(KV) * [my_tile]), concat_axis=0, split_axi...]
    all_to_all x0 -> x1, starting transfers between devices: none -> 5.11 us  [cover_run(): all_to_all(jnp.stack(axis_size(KV) * [my_tile]), concat_axis=0, split_axi...]
  transfers between devices with their start and end apart: 3 -> 4, of which waited for: 3 -> 4; matrix products, arithmetic and copies ran while one was open for 1% -> 1% of each run, Pallas kernels for 0% -> 0%
where the time goes in v1:
time: 410 us
  waiting for transfers between devices  308 us (75%)
  blocking collectives  45.5 us (11%)
  matrix products  18.5 us (5%)
  between operations  14.8 us (4%)
  local copies, waits for them, and re-layouts  8.99 us (2%)
  other arithmetic  8.67 us (2%)
  starting transfers between devices  5.42 us (1%)
    unnamed x5, waiting for transfers between devices  239 us
    all_gather x1, waiting for transfers between devices, local(): whole_rows = lax.all_gather(residual, KV_TP, axis=1, tiled=True)  61.1 us
    all_to_all x2, blocking collectives, exchange_in_order(): filled = lax.all_to_all(filled, axes[k], k, k, tiled=True)  20.4 us
    all_gather x1, blocking collectives, local(): columns = lax.all_gather(tokens, TP, axis=1, tiled=True)  13.6 us
    all_to_all x1, blocking collectives, summed_on_arrival(): lax.all_to_all(in_blocks(value, dim, count), axis, 0, 0, tiled=True)  11.6 us
  transfers between devices with their start and end apart: 4, of which 4 were waited for; matrix products, arithmetic and copies ran while one was open for 1% of the time, Pallas kernels for 0%

profile of v1, /device:TPU:0, one launch (start us, length us, event | category | flops | bytes accessed | tf_op | source)
XLA Modules:
  0.0 409.7 jit_solution(11896370815508657656)
XLA Ops:
  7.3 13.6 %all_gather.6 = bf16[256,256]{0,1:T(8,128)(2,1)S(1)} all-gather(bf16[256,32]{0,1:T(8,128)(2,1)} %param.15), channel_id=1, replica_groups=mesh['kv_0'=4,'kv_1'=4,'tp_0'=4,'tp_1'=2] {'tp_0','tp_1'}, dimensions={1}, use_global_device_ids=true | all-gather | bytes 147456 | tf_op jit(solution)/shard_map/all_gather | solution.py:107
  20.9 0.1 copy.46
  21.0 1.3 fusion.51
  22.3 1.3 fusion.49
  23.6 1.3 fusion.47
  24.9 1.3 fusion.53
  26.2 0.3 fusion.32
  26.5 1.4 concatenate.7
  28.0 0.6 dynamic-slice
  29.2 89.5 %all-reduce.5.cloned.1.call-done = f32[256,1585]{1,0:T(8,128)} async-done(((f32[256,1585]{1,0:T(8,128)}), f32[256,1585]{1,0:T(8,128)}) %all-reduce.5.cloned.1.call-update) | async-done | bytes 1623056
  118.8 0.9 fusion.43
  119.7 0.9 dynamic-slice_multiply_fusion.1
  120.6 0.1 multiply_reduce_fusion.1
  120.8 0.1 fusion.64
  120.8 0.1 broadcast_multiply_fusion
  121.0 0.1 multiply_reduce_fusion
  121.1 0.1 multiply_bitcast_fusion
  121.2 0.9 dynamic-slice_multiply_fusion.5
  122.1 0.1 add_divide_fusion
  122.3 4.8 %fusion.3 = f32[16,3,1,128]{3,2,1,0:T(1,128)S(1)} fusion(f32[16,3,128,128]{3,2,1,0:T(8,128)} %param.25, f32[16,3]{1,0:T(8,128)S(1)} %get-tuple-element.15, f32[16,3,128,1]{2,1,0,3:T(4,128)S(1)} %fusion.64), kind=kOutput, calls=%fused_computation.6 | convolution fusion | flops 10223616 | bytes 3195072 | tf_op jit(solution)/shard_map/bhkv,bhk->bhv/dot_general | solution.py:145
  127.1 1.1 multiply_add_fusion
  128.3 1.7 copy-done.3
  129.9 2.8 fusion.36
  132.7 0.1 fusion.28
  132.8 0.1 fusion.31
  132.9 0.7 stack.2
  133.6 5.1 %all-to-all-start = ((bf16[16,16,384]{2,1,0:T(8,128)(2,1)}), bf16[16,16,384]{2,1,0:T(8,128)(2,1)S(1)}, u32[]{:S(2)}, u32[]{:S(2)}) async-start(bf16[16,16,384]{2,1,0:T(8,128)(2,1)} %stack.2), calls=%async_computation | async-start | bytes 393216 | tf_op jit(solution)/shard_map/all_to_all | solution.py:18
  138.8 0.2 copy.47
  139.0 8.1 %all-to-all-done = bf16[16,16,384]{2,1,0:T(8,128)(2,1)S(1)} async-done(((bf16[16,16,384]{2,1,0:T(8,128)(2,1)}), bf16[16,16,384]{2,1,0:T(8,128)(2,1)S(1)}, u32[]{:S(2)}, u32[]{:S(2)}) %all-to-all-start) | async-done | bytes 196640 | tf_op jit(solution)/shard_map/all_to_all | solution.py:18
  147.1 0.2 convolution_bitcast_fusion
  147.3 11.6 %all_to_all.20 = f32[8,256,32]{1,2,0:T(8,128)S(1)} all-to-all(f32[8,256,32]{1,2,0:T(8,128)S(1)} %convolution_bitcast_fusion), channel_id=1, replica_groups=mesh['kv_0'=4,'kv_1'=4,'tp_0'=4,'tp_1'=2] {'tp_0','tp_1'}, dimensions={0} | all-to-all | bytes 524288 | tf_op jit(solution)/shard_map/all_to_all | solution.py:45
  158.9 0.6 add_convert_fusion
  159.6 0.2 all-reduce.7.cloned.1.call-start
  159.8 61.1 %all-gather.2.cloned.1.call-done = bf16[256,4096]{0,1:T(8,128)(2,1)} async-done(((bf16[256,32]{0,1:T(8,128)(2,1)}), bf16[256,4096]{0,1:T(8,128)(2,1)}) %all-gather.2.cloned.1.call-update) | async-done | bytes 2097168 | tf_op jit(solution)/shard_map/all_gather | solution.py:162
  220.9 2.3 fusion
  223.2 5.3 %fusion.20 = f32[256,4096]{1,0:T(8,128)} fusion(bf16[128,4096]{1,0:T(8,128)(2,1)S(1)} %copy-done, bf16[4096,128]{1,0:T(8,128)(2,1)} %param.28, bf16[256,4096]{0,1:T(8,128)(2,1)S(1)} %copy-done.1, f32[4096]{0:T(1024)S(1)} %copy-done.7, f32[256]{0:T(256)S(1)} %add_rsqrt_fusion.3), kind=kOutput, calls=%fused_computation.16 | convolution fusion | flops 541163520 | bytes 8406016 | tf_op jit(solution)/shard_map/dot_general | solution.py:83
  228.6 1.4 constant_dynamic-slice_fusion
  230.0 1.6 copy.57
  231.6 149.0 %all-reduce.7.cloned.1.call-done = f32[256,4096]{1,0:T(8,128)} async-done(((f32[256,4096]{1,0:T(8,128)}), f32[256,4096]{1,0:T(8,128)}) %all-reduce.7.cloned.1.call-update) | async-done | bytes 4194320
  380.6 0.9 fusion.27
  381.5 0.1 reshape.91
  381.6 0.1 copy.49
  381.7 0.1 reshape.100
  381.8 3.7 all_to_all.21
  385.6 0.1 reshape.101
  385.7 0.1 copy.50
  385.8 16.7 %all_to_all.22 = bf16[64,2,2,32]{3,2,1,0:T(2,128)(2,1)S(1)} all-to-all(bf16[64,2,2,32]{3,2,1,0:T(2,128)(2,1)S(1)} %copy.50), channel_id=1, replica_groups=mesh['kv_0'=4,'kv_1'=4,'tp_0'=4,'tp_1'=2] {'kv_0','kv_1','tp_0'}, dimensions={0} | all-to-all | bytes 32768 | tf_op jit(solution)/shard_map/all_to_all | solution.py:59
  402.5 0.7 copy.51
  (43 shorter events, 0.4 us)
Async XLA Ops:
  7.2 216.0 %copy-start = (bf16[128,4096]{1,0:T(8,128)(2,1)S(1)}, bf16[128,4096]{1,0:T(8,128)(2,1)}, u32[]{:S(2)}) copy-start(bf16[128,4096]{1,0:T(8,128)(2,1)} %param.29) | copy-start | bytes 3145732
  7.2 19.0 %copy-start.6 = (f32[256]{0:T(256)S(1)}, f32[256]{0:T(256)}, u32[]{:S(2)}) copy-start(f32[256]{0:T(256)} %param.16) | copy-start | bytes 3076
  7.2 19.0 %copy-start.8 = (bf16[256,24]{0,1:T(8,128)(2,1)S(1)}, bf16[256,24]{0,1:T(8,128)(2,1)}, u32[]{:S(2)}) copy-start(bf16[256,24]{0,1:T(8,128)(2,1)} %param.22) | copy-start | bytes 36868
  7.2 19.0 %copy-start.9 = (bf16[256,24]{0,1:T(8,128)(2,1)S(1)}, bf16[256,24]{0,1:T(8,128)(2,1)}, u32[]{:S(2)}) copy-start(bf16[256,24]{0,1:T(8,128)(2,1)} %param.21) | copy-start | bytes 36868
  7.2 111.6 %all-reduce.5.cloned.1.call-start = ((), (), s32[]{:S(2)}) async-start(), calls=%async_computation.5 | async-start | bytes 3407872
  24.9 3.1 copy-start.11
  24.9 3.1 copy-start.12
  121.2 5.9 %copy-start.2 = (f32[16,3,128,128]{3,2,1,0:T(8,128)S(1)}, f32[16,3,128,128]{3,2,1,0:T(8,128)}, u32[]{:S(2)}) copy-start(f32[16,3,128,128]{3,2,1,0:T(8,128)} %param.25) | copy-start | bytes 9437188
  128.3 1.7 copy-start.3
  129.9 2.9 copy-start.10
  129.9 8.9 %copy-start.4 = (bf16[384,256]{1,0:T(8,128)(2,1)S(1)}, bf16[384,256]{1,0:T(8,128)(2,1)}, u32[]{:S(2)}) copy-start(bf16[384,256]{1,0:T(8,128)(2,1)} %param.26) | copy-start | bytes 589828
  129.9 29.0 %copy-start.5 = (bf16[256,32]{0,1:T(8,128)(2,1)S(1)}, bf16[256,32]{0,1:T(8,128)(2,1)}, u32[]{:S(2)}) copy-start(bf16[256,32]{0,1:T(8,128)(2,1)} %param.15) | copy-start | bytes 49156
  132.7 90.5 %copy-start.7 = (f32[4096]{0:T(1024)S(1)}, f32[4096]{0:T(1024)}, u32[]{:S(2)}) copy-start(f32[4096]{0:T(1024)} %param.27) | copy-start | bytes 49156
  133.6 13.5 %all-to-all-start = ((bf16[16,16,384]{2,1,0:T(8,128)(2,1)}), bf16[16,16,384]{2,1,0:T(8,128)(2,1)S(1)}, u32[]{:S(2)}, u32[]{:S(2)}) async-start(bf16[16,16,384]{2,1,0:T(8,128)(2,1)} %stack.2), calls=%async_computation | async-start | bytes 393216 | tf_op jit(solution)/shard_map/all_to_all | solution.py:18
  138.7 82.1 %all-gather.2.cloned.1.call-start = ((), (), s32[]{:S(2)}) async-start(), calls=%async_computation.4 | async-start | bytes 2113536 | tf_op jit(solution)/shard_map/all_gather | solution.py:162
  159.6 221.0 %all-reduce.7.cloned.1.call-start = ((), (), s32[]{:S(2)}) async-start(), calls=%async_computation.6 | async-start | bytes 8388608
  220.9 2.3 copy-start.1
Sparse Core Ops, SparseCore 0:
  28.1 90.6 all-reduce.4
  159.7 61.1 all-gather.1
  228.7 151.8 all-reduce.6
